TPU v7x, 32 devices: a whole 2x2x4 slice. The times are simulated.
32 devices in a mesh: fs: 16 (over z, y, x), tp: 2 (over core).
Axes of the slice: x: 2, y: 2, z: 4, core: 2. Of those that a mesh axis runs over, the one named last changes fastest.
Arguments:
- tokens: bfloat16 [3072, 2048], P('fs'), may hold values from -6 to 6
- route_ids: int32 [3072, 2], P('fs'), may hold values from 0 to 7, all different within a row; in each aligned block of 192 rows (0 to 191, 192 to 383, ...) at most 96 rows name the same one
- route_logits: float32 [3072, 2], P('fs'), may hold values from -6 to 6
- norm_gain: float32 [2048], P('fs'), may hold values from 0.1 to 1.9
- gate_weight: float32 [8, 2048, 2048], P(None, 'fs', 'tp'), may hold values from -0.125 to 0.125
- up_weight: float32 [8, 2048, 2048], P(None, 'fs', 'tp'), may hold values from -0.125 to 0.125
- down_weight: float32 [8, 2048, 2048], P(None, 'fs', 'tp'), may hold values from -0.125 to 0.125
Outputs:
- mixed: bfloat16 [3072, 2048], P('fs')
- gate_copies: bfloat16 [16, 2048, 2048], P('fs', None, 'tp')
- up_copies: bfloat16 [16, 2048, 2048], P('fs', None, 'tp')
- down_copies: bfloat16 [16, 2048, 2048], P('fs', None, 'tp')
Inputs may be any that keep to these rules, and one draw needn't show every extreme that they name: `route_ids`: each row names 2 different experts. Among the rows of one index of fs no expert is named by more than 96 rows, a bound that some of them reach.
All inputs are finite; a program needn't handle non-finite values.
Results may differ from a plain program's by a relative error of at most 0.014.
Values may be sent and summed in bfloat16 or wider, within the bound.
A program may use at most 128 MiB of HBM per device.

v0:
```python
import jax
import jax.numpy as jnp
from jax import lax
from jax.sharding import PartitionSpec as P

CAP = 96


def body(tokens, route_ids, route_logits, norm_gain, gate_weight, up_weight, down_weight):
    experts = gate_weight.shape[0]
    fs_count = lax.axis_size("fs")
    copies = fs_count // experts
    per_peer = CAP // copies
    tok_rows = tokens.shape[0]
    width = tokens.shape[1]
    scaled_gain = norm_gain[None, :, None]
    gate_send = jnp.repeat((scaled_gain * gate_weight).astype(jnp.bfloat16), copies, axis=0)
    up_send = jnp.repeat((scaled_gain * up_weight).astype(jnp.bfloat16), copies, axis=0)
    down_send = jnp.repeat(down_weight.astype(jnp.bfloat16), copies, axis=0)
    gate_new, up_new, down_new = (
        lax.all_to_all(gate_send, "fs", split_axis=0, concat_axis=1, tiled=True),
        lax.all_to_all(up_send, "fs", split_axis=0, concat_axis=1, tiled=True),
        lax.all_to_all(down_send, "fs", split_axis=0, concat_axis=1, tiled=True),
    )
    values = tokens.astype(jnp.float32)
    center = jnp.mean(values, axis=1, keepdims=True)
    spread = jnp.mean(jnp.square(values - center), axis=1, keepdims=True)
    normed = ((values - center) * lax.rsqrt(spread + 1e-06)).astype(jnp.bfloat16)
    flat_ids = route_ids.reshape(-1)
    onehot_table = (flat_ids[:, None] == jnp.arange(experts, dtype=jnp.int32)[None, :]).astype(
        jnp.int32
    )
    before = jnp.cumsum(onehot_table, axis=0) - onehot_table
    order_rank = jnp.sum(before * onehot_table, axis=1)
    dest_flat = (flat_ids * copies + order_rank % copies) * per_peer + order_rank // copies
    owners = jnp.arange(flat_ids.shape[0], dtype=jnp.int32) // route_ids.shape[1]
    slot_token = jnp.full((experts * CAP,), tok_rows, jnp.int32).at[dest_flat].set(owners)
    padded = jnp.concatenate([normed, jnp.zeros((1, width), jnp.bfloat16)], axis=0)
    send_rows = padded[slot_token].reshape(fs_count, per_peer, width)
    gate_matrix = gate_new[0]
    up_matrix = up_new[0]
    col_count = width // lax.axis_size("tp")
    col_start = lax.axis_index("tp") * col_count
    own_cols = lax.dynamic_slice_in_dim(send_rows, col_start, col_count, 2)
    arrived = lax.all_to_all(own_cols, "fs", split_axis=0, concat_axis=0, tiled=True).reshape(
        -1, col_count
    )
    piece = lax.all_gather(arrived, "tp", axis=1, tiled=True)
    gate_act = jnp.dot(piece, gate_matrix, preferred_element_type=jnp.float32)
    up_act = jnp.dot(piece, up_matrix, preferred_element_type=jnp.float32)
    hidden = (jax.nn.silu(gate_act) * up_act).astype(jnp.bfloat16)
    partial_value = jnp.einsum("rf,df->rd", hidden, down_new[0], preferred_element_type=jnp.float32)
    share = lax.psum_scatter(
        partial_value.astype(jnp.bfloat16), "tp", scatter_dimension=1, tiled=True
    )
    back_part = lax.all_to_all(
        share.reshape(fs_count, per_peer, col_count), "fs", split_axis=0, concat_axis=0, tiled=True
    )
    returned = lax.all_gather(back_part, "tp", axis=2, tiled=True).reshape(-1, width)
    picked = returned[dest_flat].reshape(tok_rows, route_ids.shape[1], width).astype(jnp.float32)
    first_weight = jax.nn.sigmoid(route_logits[:, 0] - route_logits[:, 1])
    second_weight = jax.nn.sigmoid(route_logits[:, 1] - route_logits[:, 0])
    mixed = (first_weight[:, None] * picked[:, 0] + second_weight[:, None] * picked[:, 1]).astype(
        jnp.bfloat16
    )
    return (mixed, gate_new, up_new, down_new)


def solution(mesh):
    return jax.shard_map(
        body,
        mesh=mesh,
        in_specs=(
            P("fs", None),
            P("fs", None),
            P("fs", None),
            P("fs"),
            P(None, "fs", "tp"),
            P(None, "fs", "tp"),
            P(None, "fs", "tp"),
        ),
        out_specs=(P("fs", None), P("fs", None, "tp"), P("fs", None, "tp"), P("fs", None, "tp")),
        check_vma=False,
    )
```

profile of v0, /device:TPU:1, one launch (start us, length us, event | category | flops | bytes accessed | tf_op | source)
XLA Modules:
  0.0 481.9 jit_solution(4758031760930865264)
XLA Ops:
  7.2 0.8 copy.14
  8.0 0.1 eq.31
  8.1 0.1 eq.27
  8.3 0.7 broadcast_multiply_fusion
  9.0 0.9 reduce-window.6
  9.8 0.2 slice_reduce_fusion
  10.1 0.1 copy.13
  10.2 0.1 mul.92
  10.4 0.1 fusion.9
  10.5 2.9 scatter_custom_fusion
  13.4 1.3 convert_reduce_fusion
  14.8 1.5 fusion.2
  16.3 1.6 fusion.3
  17.9 0.1 concatenate.3
  18.0 4.2 gather_fusion
  22.2 2.7 constant_dynamic-slice_fusion
  24.9 7.4 %all-to-all-start = ((bf16[16,48,1024]{2,1,0:T(8,128)(2,1)}), bf16[16,48,1024]{2,1,0:T(8,128)(2,1)}, u32[]{:S(2)}, u32[]{:S(2)}) async-start(bf16[16,48,1024]{2,1,0:T(8,128)(2,1)} %constant_dynamic-slice_fusion), calls=%async_computation | async-start | bytes 3145728 | tf_op jit(solution)/shard_map/all_to_all | solution.py:45
  32.4 6.1 %multiply_convert_fusion = (bf16[8,128,1024]{2,1,0:T(8,128)(2,1)S(1)}, bf16[8,128,1024]{2,1,0:T(8,128)(2,1)}) fusion(f32[8,128,1024]{2,1,0:T(8,128)} %param.12, f32[128]{0:T(128)S(1)} %copy-done.2, f32[8,128,1024]{2,1,0:T(8,128)} %param.11), kind=kLoop, calls=%fused_computation.3 | loop fusion | flops 4194304 | bytes 12583424 | tf_op jit(solution)/shard_map/convert_element_type | solution.py:18
  38.5 25.5 %all-to-all-done = bf16[16,48,1024]{2,1,0:T(8,128)(2,1)} async-done(((bf16[16,48,1024]{2,1,0:T(8,128)(2,1)}), bf16[16,48,1024]{2,1,0:T(8,128)(2,1)}, u32[]{:S(2)}, u32[]{:S(2)}) %all-to-all-start) | async-done | bytes 1572896 | tf_op jit(solution)/shard_map/all_to_all | solution.py:45
  64.0 2.1 broadcast_in_dim.12
  66.2 101.4 %all_to_all.46 = bf16[16,128,1024]{2,1,0:T(8,128)(2,1)} all-to-all(bf16[16,128,1024]{2,1,0:T(8,128)(2,1)S(1)} %bitcast.48), channel_id=1, replica_groups=mesh['fs'=16,'tp'=2] {'fs'}, dimensions={0} | all-to-all | bytes 8388608 | tf_op jit(solution)/shard_map/all_to_all | solution.py:21
  167.6 2.6 broadcast_in_dim.13
  170.2 5.2 %all-to-all-start.2 = ((bf16[16,128,1024]{2,1,0:T(8,128)(2,1)}), bf16[16,128,1024]{2,1,0:T(8,128)(2,1)}, u32[]{:S(2)}, u32[]{:S(2)}) async-start(bf16[16,128,1024]{2,1,0:T(8,128)(2,1)} %bitcast.47), calls=%async_computation.2 | async-start | bytes 8388608 | tf_op jit(solution)/shard_map/all_to_all | solution.py:22
  175.4 2.5 convert_element_type.44
  177.9 75.7 %all-to-all-done.2 = bf16[16,128,1024]{2,1,0:T(8,128)(2,1)} async-done(((bf16[16,128,1024]{2,1,0:T(8,128)(2,1)}), bf16[16,128,1024]{2,1,0:T(8,128)(2,1)}, u32[]{:S(2)}, u32[]{:S(2)}) %all-to-all-start.2) | async-done | bytes 4194336 | tf_op jit(solution)/shard_map/all_to_all | solution.py:22
  253.6 2.6 broadcast_in_dim.28
  256.2 19.4 %all-to-all-start.3 = ((bf16[16,128,1024]{2,1,0:T(8,128)(2,1)}), bf16[16,128,1024]{2,1,0:T(8,128)(2,1)}, u32[]{:S(2)}, u32[]{:S(2)}) async-start(bf16[16,128,1024]{2,1,0:T(8,128)(2,1)} %bitcast.46), calls=%async_computation.3 | async-start | bytes 8388608 | tf_op jit(solution)/shard_map/all_to_all | solution.py:23
  275.6 0.0 all-gather.3.cloned.1.call-start
  275.7 0.7 all-gather.3.cloned.1.call-update
  276.4 0.2 reduce-scatter.2.cloned.1.call-start
  276.6 16.2 %all-gather.3.cloned.1.call-done = bf16[768,2048]{1,0:T(8,128)(2,1)} async-done(((bf16[768,1024]{1,0:T(8,128)(2,1)}), bf16[768,2048]{1,0:T(8,128)(2,1)}) %all-gather.3.cloned.1.call-update) | async-done | bytes 3145744 | tf_op jit(solution)/shard_map/all_gather | solution.py:48
  292.8 8.2 %fusion.20 = f32[768,1024]{1,0:T(8,128)} fusion(bf16[768,2048]{1,0:T(8,128)(2,1)} %all-gather.3.cloned.1.call-done, bf16[2048,1024]{1,0:T(8,128)(2,1)} %bitcast.44), kind=kOutput, calls=%fused_computation.54 | convolution fusion | flops 3221225472 | bytes 10485760 | tf_op jit(solution)/shard_map/dot_general | solution.py:49
  301.0 52.4 %all-to-all-done.3 = bf16[16,128,1024]{2,1,0:T(8,128)(2,1)} async-done(((bf16[16,128,1024]{2,1,0:T(8,128)(2,1)}), bf16[16,128,1024]{2,1,0:T(8,128)(2,1)}, u32[]{:S(2)}, u32[]{:S(2)}) %all-to-all-start.3) | async-done | bytes 4194336 | tf_op jit(solution)/shard_map/all_to_all | solution.py:23
  353.4 12.5 %convolution_convert_fusion = bf16[768,2048]{1,0:T(8,128)(2,1)} fusion(bf16[2048,1024]{1,0:T(8,128)(2,1)} %bitcast.10, f32[768,1024]{1,0:T(8,128)} %fusion.20, bf16[768,2048]{1,0:T(8,128)(2,1)} %all-gather.3.cloned.1.call-done, bf16[2048,1024]{1,0:T(8,128)(2,1)} %bitcast.8), kind=kOutput, calls=%fused_computation.5 | convolution fusion | flops 6448742400 | bytes 17825792 | tf_op jit(solution)/shard_map/rf,df->rd/dot_general | solution.py:52
  365.9 0.0 reduce-scatter.2.cloned.1.call-update
  365.9 0.0 copy-start.1
  365.9 0.0 all-gather.5.cloned.1.call-start
  366.0 27.1 %reduce-scatter.2.cloned.1.call-done = bf16[768,1024]{1,0:T(8,128)(2,1)} async-done(((bf16[768,2048]{1,0:T(8,128)(2,1)}), bf16[768,1024]{1,0:T(8,128)(2,1)}) %reduce-scatter.2.cloned.1.call-update) | async-done | bytes 1572880 | tf_op jit(solution)/shard_map/reduce_scatter | solution.py:53
  393.0 42.4 %all_to_all.47 = bf16[16,48,1024]{2,1,0:T(8,128)(2,1)} all-to-all(bf16[16,48,1024]{2,1,0:T(8,128)(2,1)} %bitcast.50), channel_id=1, replica_groups=mesh['fs'=16,'tp'=2] {'fs'}, dimensions={0} | all-to-all | bytes 3145728 | tf_op jit(solution)/shard_map/all_to_all | solution.py:56
  435.4 0.0 all-gather.5.cloned.1.call-update
  435.5 13.0 %all-gather.5.cloned.1.call-done = bf16[16,48,2048]{2,1,0:T(8,128)(2,1)} async-done(((bf16[16,48,1024]{2,1,0:T(8,128)(2,1)}), bf16[16,48,2048]{2,1,0:T(8,128)(2,1)}) %all-gather.5.cloned.1.call-update) | async-done | bytes 3145744 | tf_op jit(solution)/shard_map/all_gather | solution.py:59
  448.4 7.3 %gather_fusion.1 = bf16[384,2048]{1,0:T(8,128)(2,1)} fusion(bf16[768,2048]{1,0:T(8,128)(2,1)} %bitcast.43, s32[1024]{0:T(1024)S(1)} %pad_clamp_fusion), kind=kCustom, calls=%fused_computation.1 | custom fusion | bytes 3147264 | tf_op jit(solution)/shard_map/gather | solution.py:60
  455.8 3.4 reshape.184
  459.2 2.4 fusion.19
  461.6 2.5 fusion.6
  464.1 2.0 copy.35
  466.1 4.6 copy.36
  470.8 4.6 copy.37
  (15 shorter events, 0.1 us)
Async XLA Ops:
  22.2 10.2 %copy-start.2 = (f32[128]{0:T(128)S(1)}, f32[128]{0:T(128)}, u32[]{:S(2)}) copy-start(f32[128]{0:T(128)} %param.10) | copy-start | bytes 1540
  24.9 39.1 %all-to-all-start = ((bf16[16,48,1024]{2,1,0:T(8,128)(2,1)}), bf16[16,48,1024]{2,1,0:T(8,128)(2,1)}, u32[]{:S(2)}, u32[]{:S(2)}) async-start(bf16[16,48,1024]{2,1,0:T(8,128)(2,1)} %constant_dynamic-slice_fusion), calls=%async_computation | async-start | bytes 3145728 | tf_op jit(solution)/shard_map/all_to_all | solution.py:45
  170.2 83.4 %all-to-all-start.2 = ((bf16[16,128,1024]{2,1,0:T(8,128)(2,1)}), bf16[16,128,1024]{2,1,0:T(8,128)(2,1)}, u32[]{:S(2)}, u32[]{:S(2)}) async-start(bf16[16,128,1024]{2,1,0:T(8,128)(2,1)} %bitcast.47), calls=%async_computation.2 | async-start | bytes 8388608 | tf_op jit(solution)/shard_map/all_to_all | solution.py:22
  256.2 97.2 %all-to-all-start.3 = ((bf16[16,128,1024]{2,1,0:T(8,128)(2,1)}), bf16[16,128,1024]{2,1,0:T(8,128)(2,1)}, u32[]{:S(2)}, u32[]{:S(2)}) async-start(bf16[16,128,1024]{2,1,0:T(8,128)(2,1)} %bitcast.46), calls=%async_computation.3 | async-start | bytes 8388608 | tf_op jit(solution)/shard_map/all_to_all | solution.py:23
  275.6 17.1 %all-gather.3.cloned.1.call-start = ((), (), s32[]{:S(2)}) async-start(), calls=%async_computation.6 | async-start | bytes 4718592 | tf_op jit(solution)/shard_map/all_gather | solution.py:48
  276.4 116.7 %reduce-scatter.2.cloned.1.call-start = ((), (), s32[]{:S(2)}) async-start(), calls=%async_computation.7 | async-start | bytes 4718592 | tf_op jit(solution)/shard_map/reduce_scatter | solution.py:53
  365.9 69.5 %copy-start.1 = (f32[192,2]{0,1:T(2,128)S(1)}, f32[192,2]{0,1:T(2,128)}, u32[]{:S(2)}) copy-start(f32[192,2]{0,1:T(2,128)} %param.9) | copy-start | bytes 4612
  365.9 82.5 %all-gather.5.cloned.1.call-start = ((), (), s32[]{:S(2)}) async-start(), calls=%async_computation.8 | async-start | bytes 4718592 | tf_op jit(solution)/shard_map/all_gather | solution.py:59
  459.2 4.9 %copy-start = (bf16[16,128,1024]{2,1,0:T(8,128)(2,1)S(1)}, bf16[16,128,1024]{2,1,0:T(8,128)(2,1)}, u32[]{:S(2)}) copy-start(bf16[16,128,1024]{2,1,0:T(8,128)(2,1)} %all_to_all.46) | copy-start | bytes 12582916
Sparse Core Ops, SparseCore 0:
  278.0 14.7 all-gather.2
  366.0 26.9 reduce-scatter.1
  435.6 12.8 all-gather.4
where the time goes:
time: 483 us; the launch traced here: 482 us
  waiting for transfers between devices  211 us (44%)
  blocking collectives  144 us (30%)
  local copies, waits for them, and re-layouts  43.4 us (9%)
  starting transfers between devices  32.3 us (7%)
  matrix products  20.8 us (4%)
  other arithmetic  17.3 us (4%)
  between operations  13.9 us (3%)
    all_to_all x1, blocking collectives, body(): lax.all_to_all(gate_send, 'fs', split_axis=0, concat_axis=1, tiled=True)  101 us
    all_to_all x1, waiting for transfers between devices, body(): lax.all_to_all(up_send, 'fs', split_axis=0, concat_axis=1, tiled=True)  75.7 us
    all_to_all x1, waiting for transfers between devices, body(): lax.all_to_all(down_send, 'fs', split_axis=0, concat_axis=1, tiled=True)  52.4 us
    all_to_all x1, blocking collectives, body(): lax.all_to_all(share.reshape(fs_count, per_peer, col_count), 'fs', split_...  42.4 us
    reduce_scatter x1, waiting for transfers between devices, body(): lax.psum_scatter(partial_value.astype(jnp.bfloat16), 'tp', scatter_dimens...  27.1 us
    all_to_all x1, waiting for transfers between devices, body(): lax.all_to_all(own_cols, 'fs', split_axis=0, concat_axis=0, tiled=True)  25.5 us
    all_to_all x1, starting transfers between devices, body(): lax.all_to_all(down_send, 'fs', split_axis=0, concat_axis=1, tiled=True)  19.4 us
    all_gather x1, waiting for transfers between devices, body(): piece = lax.all_gather(arrived, 'tp', axis=1, tiled=True)  16.2 us
  transfers between devices with their start and end apart: 6, of which 6 were waited for; matrix products, arithmetic and copies ran while one was open for 4% of the time, Pallas kernels for 0%

commit v1 on v0

v1 whole, which is shorter than its diff:
```python
import functools

import jax
import jax.numpy as jnp
from jax import lax
from jax.experimental import pallas as pl
from jax.experimental.pallas import tpu as pltpu
from jax.sharding import PartitionSpec as P

CAP = 96
MESH = pl.DeviceIdType.MESH
BF16 = jnp.bfloat16
F32 = jnp.float32


def handoff(
    experts,
    copies,
    tps,
    tok,
    gain,
    gate_in,
    up_in,
    down_in,
    gate_out,
    up_out,
    down_out,
    back_out,
    stage,
    send,
    full,
    rows_in,
    hidden,
    part,
    part_in,
    share,
    back,
    load_sem,
    w_send,
    w_recv,
    r_send,
    r_recv,
    t_send,
    t_recv,
    tx_send,
    tx_recv,
    p_send,
    p_recv,
    b_send,
    b_recv,
    bx_send,
    bx_recv,
    out_sem,
    tok_sem,
):
    shard, cols = stage.shape[2], stage.shape[3]
    width = rows_in.shape[1]
    block = tok.shape[1]
    chunk_f = min(256, cols)
    chunk_w = min(256, block)
    n_f, n_w = cols // chunk_f, block // chunk_w
    me = lax.axis_index("fs")
    tp = lax.axis_index("tp")
    group = lax.div(me, copies)
    lane = lax.rem(me, copies)
    weights = (gate_in, up_in, down_in)
    outs = (gate_out, up_out, down_out)

    def ahead(d):
        return lax.rem(group + d, experts)

    def behind(d):
        return lax.rem(group + experts - d, experts)

    def twin(c):
        return lax.rem(lane + c, copies)

    def mate(p):
        return lax.rem(tp + p, tps)

    def slots(e):
        return pl.ds(pl.multiple_of(e * CAP, 32), CAP)

    def own_cols(q, j=0, size=block):
        return pl.ds(pl.multiple_of(q * block + j * chunk_w, 128), size)

    def shard_rows(g, c):
        return pl.ds(pl.multiple_of((g * copies + c) * shard, 32), shard)

    def loop(lo, hi, body):
        def step(i, carry):
            body(i)
            return carry

        lax.fori_loop(lo, hi, step, 0)

    def remote(src, dst, s_sem, r_sem, fs_to, tp_to):
        return pltpu.make_async_remote_copy(
            src_ref=src,
            dst_ref=dst,
            send_sem=s_sem,
            recv_sem=r_sem,
            device_id=(fs_to, tp_to),
            device_id_type=MESH,
        )

    def load(m, h):
        return pltpu.make_async_copy(weights[m].at[h], stage.at[m, h], load_sem.at[m, h])

    def direct(m, h, s):
        return remote(
            send.at[m, h],
            full.at[m, shard_rows(s, lane)],
            w_send.at[m, h],
            w_recv.at[m, s],
            h * copies + lane,
            tp,
        )

    def relay(m, s, c, to):
        return remote(
            full.at[m, shard_rows(s, c)],
            full.at[m, shard_rows(s, c)],
            r_send.at[m, s, to],
            r_recv.at[m, s, c],
            group * copies + to,
            tp,
        )

    def dispatch(h, s):
        return remote(
            tok.at[slots(h)],
            rows_in.at[slots(s), own_cols(tp)],
            t_send.at[h],
            t_recv.at[s],
            h * copies + lane,
            tp,
        )

    def spread(s, q, p):
        return remote(
            rows_in.at[slots(s), own_cols(q)],
            rows_in.at[slots(s), own_cols(q)],
            tx_send.at[s, p],
            tx_recv.at[s, p],
            me,
            mate(p),
        )

    def partial(p, j):
        where = pl.ds(pl.multiple_of(j * chunk_w, 128), chunk_w)
        return remote(
            part.at[p - 1, :, where],
            part_in.at[p - 1, :, where],
            p_send.at[p, j],
            p_recv.at[p, j],
            me,
            mate(p),
        )

    def give(s, e, j):
        where = pl.ds(pl.multiple_of(j * chunk_w, 128), chunk_w)
        return remote(
            share.at[slots(s), where],
            back.at[slots(e), own_cols(tp, j, chunk_w)],
            b_send.at[s, j],
            b_recv.at[e, j],
            s * copies + lane,
            tp,
        )

    def fan(e, q, j, p):
        return remote(
            back.at[slots(e), own_cols(q, j, chunk_w)],
            back.at[slots(e), own_cols(q, j, chunk_w)],
            bx_send.at[e, j, p],
            bx_recv.at[e, j, p],
            me,
            mate(p),
        )

    for m in range(3):
        loop(0, experts, lambda d, m=m: load(m, ahead(d)).start())
    tok_copy = pltpu.make_async_copy(
        tok.at[slots(group)], rows_in.at[slots(group), own_cols(tp)], tok_sem
    )
    tok_copy.start()

    barrier = pltpu.get_barrier_semaphore()
    for d in range(1, experts):
        pl.semaphore_signal(
            barrier, inc=1, device_id=(ahead(d) * copies + lane, tp), device_id_type=MESH
        )
    for c in range(1, copies):
        pl.semaphore_signal(
            barrier, inc=1, device_id=(group * copies + twin(c), tp), device_id_type=MESH
        )
    for p in range(1, tps):
        pl.semaphore_signal(barrier, inc=1, device_id=(me, mate(p)), device_id_type=MESH)
    pl.semaphore_wait(barrier, experts + copies + tps - 3)

    loop(1, experts, lambda d: dispatch(ahead(d), group).start())

    def rounded(m, h):
        load(m, h).wait()
        value = stage[m, h]
        if m < 2:
            value = gain[...] * value
        return value.astype(BF16)

    for m in range(3):
        full[m, shard_rows(group, lane)] = rounded(m, group)
    for m in range(3):
        def convert(d, m=m):
            send[m, ahead(d)] = rounded(m, ahead(d))

            @pl.when(d > 1)
            def _():
                direct(m, ahead(d - 1), group).start()

        loop(1, experts, convert)
        for c in range(1, copies):
            relay(m, group, lane, twin(c)).start()
        direct(m, ahead(experts - 1), group).start()

    tok_copy.wait()
    for p in range(1, tps):
        spread(group, tp, p).start()

    def spread_step(d):
        s = behind(d)
        dispatch(s, s).wait_recv()
        for p in range(1, tps):
            spread(s, tp, p).start()

    def relay_step(m, d):
        s = behind(d)
        direct(m, s, s).wait_recv()
        for c in range(1, copies):
            relay(m, s, lane, twin(c)).start()

    def relay_wait(m, s):
        for c in range(1, copies):
            relay(m, s, twin(c), lane).wait_recv()

    def out_copy(m):
        return pltpu.make_async_copy(full.at[m], outs[m].at[0], out_sem.at[m])

    loop(1, experts, spread_step)
    loop(1, experts, lambda d: relay_step(0, d))
    loop(1, experts, lambda d: relay_step(1, d))
    early = experts - n_f
    loop(1, early, lambda d: relay_step(2, d))

    def spread_wait(s):
        for p in range(1, tps):
            spread(s, mate(tps - p), p).wait_recv()

    loop(0, experts, spread_wait)
    for m in range(2):
        loop(0, experts, lambda s, m=m: relay_wait(m, s))
        out_copy(m).start()

    def gate_up(c):
        relay_step(2, early + c)
        where = pl.ds(pl.multiple_of(c * chunk_f, 128), chunk_f)
        gate = jnp.dot(rows_in[...], full[0, :, where], preferred_element_type=F32)
        up = jnp.dot(rows_in[...], full[1, :, where], preferred_element_type=F32)
        hidden[:, where] = (gate / (1.0 + jnp.exp(-gate)) * up).astype(BF16)

    loop(0, n_f, gate_up)
    loop(0, experts, lambda s: relay_wait(2, s))
    out_copy(2).start()

    def down(q, j):
        rows = full[2, own_cols(q, j, chunk_w), :]
        return lax.dot_general(
            hidden[...], rows, (((1,), (1,)), ((), ())), preferred_element_type=F32
        ).astype(BF16)

    for p in range(1, tps):
        def partial_step(j, p=p):
            where = pl.ds(pl.multiple_of(j * chunk_w, 128), chunk_w)
            part[p - 1, :, where] = down(mate(p), j)
            partial(p, j).start()

        loop(0, n_w, partial_step)

    def share_step(j):
        where = pl.ds(pl.multiple_of(j * chunk_w, 128), chunk_w)
        total = down(tp, j).astype(F32)
        for p in range(1, tps):
            partial(p, j).wait_recv()
            total = total + part_in[p - 1, :, where].astype(F32)
        share[:, where] = total.astype(BF16)
        back[slots(group), own_cols(tp, j, chunk_w)] = share[slots(group), where]
        loop(1, experts, lambda d: give(behind(d), group, j).start())
        for p in range(1, tps):
            fan(group, tp, j, p).start()

    loop(0, n_w, share_step)

    def back_step(j):
        def one(d):
            e = ahead(d)
            give(e, e, j).wait_recv()
            for p in range(1, tps):
                fan(e, tp, j, p).start()

        loop(1, experts, one)

    loop(0, n_w, back_step)

    def back_wait(j):
        def one(e):
            for p in range(1, tps):
                fan(e, mate(tps - p), j, p).wait_recv()

        loop(0, experts, one)

    loop(0, n_w, back_wait)
    last = pltpu.make_async_copy(back, back_out, tok_sem)
    last.start()

    loop(1, experts, lambda d: dispatch(ahead(d), group).wait_send())
    for m in range(3):
        loop(1, experts, lambda d, m=m: direct(m, ahead(d), group).wait_send())

        def relays(s, m=m):
            for c in range(1, copies):
                relay(m, s, lane, twin(c)).wait_send()

        loop(0, experts, relays)
        out_copy(m).wait()

    def spreads(s):
        for p in range(1, tps):
            spread(s, tp, p).wait_send()

    loop(0, experts, spreads)

    def tail(j):
        for p in range(1, tps):
            partial(p, j).wait_send()
        loop(1, experts, lambda d: give(behind(d), group, j).wait_send())

        def fans(e):
            for p in range(1, tps):
                fan(e, tp, j, p).wait_send()

        loop(0, experts, fans)

    loop(0, n_w, tail)
    last.wait()


def body(tokens, route_ids, route_logits, norm_gain, gate_weight, up_weight, down_weight):
    experts, shard, cols = gate_weight.shape
    fs_count, tps = lax.axis_size("fs"), lax.axis_size("tp")
    copies = fs_count // experts
    tok_rows, width = tokens.shape
    block = width // tps
    n_slots = experts * CAP
    depth = shard * fs_count

    values = tokens.astype(F32)
    center = jnp.mean(values, axis=1, keepdims=True)
    spread = jnp.mean(jnp.square(values - center), axis=1, keepdims=True)
    normed = ((values - center) * lax.rsqrt(spread + 1e-06)).astype(BF16)

    expert_ids = jnp.arange(experts, dtype=jnp.int32)[None, :]
    hit = [route_ids[:, k : k + 1] == expert_ids for k in range(2)]
    named = (hit[0] | hit[1]).astype(BF16)
    order = jnp.arange(tok_rows, dtype=jnp.int32)
    lower = (order[None, :] < order[:, None]).astype(BF16)
    rank = jnp.dot(lower, named, preferred_element_type=F32).astype(jnp.int32)
    place = expert_ids * CAP + rank
    slot = [jnp.sum(jnp.where(hit[k], place, 0), axis=1) for k in range(2)]
    slot_ids = jnp.arange(n_slots, dtype=jnp.int32)
    scatter = (
        (slot_ids[:, None] == slot[0][None, :]) | (slot_ids[:, None] == slot[1][None, :])
    ).astype(BF16)
    mine = lax.dynamic_slice_in_dim(normed, lax.axis_index("tp") * block, block, 1)
    tok = jnp.dot(scatter, mine, preferred_element_type=F32).astype(BF16)

    n_w = block // min(256, block)
    dma = pltpu.SemaphoreType.DMA
    anywhere = pl.BlockSpec(memory_space=pl.ANY)
    copy_shape = jax.ShapeDtypeStruct((1, depth, cols), BF16)
    gate_new, up_new, down_new, returned = pl.pallas_call(
        functools.partial(handoff, experts, copies, tps),
        out_shape=(
            copy_shape,
            copy_shape,
            copy_shape,
            jax.ShapeDtypeStruct((n_slots, width), BF16),
        ),
        in_specs=[anywhere, pl.BlockSpec(memory_space=pltpu.VMEM)] + [anywhere] * 3,
        out_specs=(anywhere,) * 4,
        scratch_shapes=[
            pltpu.VMEM((3, experts, shard, cols), F32),
            pltpu.VMEM((3, experts, shard, cols), BF16),
            pltpu.VMEM((3, depth, cols), BF16),
            pltpu.VMEM((n_slots, width), BF16),
            pltpu.VMEM((n_slots, cols), BF16),
            pltpu.VMEM((tps - 1, n_slots, block), BF16),
            pltpu.VMEM((tps - 1, n_slots, block), BF16),
            pltpu.VMEM((n_slots, block), BF16),
            pltpu.VMEM((n_slots, width), BF16),
            dma((3, experts)),
            dma((3, experts)),
            dma((3, experts)),
            dma((3, experts, copies)),
            dma((3, experts, copies)),
            dma((experts,)),
            dma((experts,)),
            dma((experts, tps)),
            dma((experts, tps)),
            dma((tps, n_w)),
            dma((tps, n_w)),
            dma((experts, n_w)),
            dma((experts, n_w)),
            dma((experts, n_w, tps)),
            dma((experts, n_w, tps)),
            dma((3,)),
            dma,
        ],
        compiler_params=pltpu.CompilerParams(
            collective_id=0, has_side_effects=True, vmem_limit_bytes=64 * 1024 * 1024 - 65536
        ),
        name="handoff",
    )(tok, norm_gain[:, None], gate_weight, up_weight, down_weight)

    picked = [
        jnp.dot(
            (slot[k][:, None] == slot_ids[None, :]).astype(BF16),
            returned,
            preferred_element_type=F32,
        )
        for k in range(2)
    ]
    first_weight = jax.nn.sigmoid(route_logits[:, 0] - route_logits[:, 1])
    second_weight = jax.nn.sigmoid(route_logits[:, 1] - route_logits[:, 0])
    mixed = (first_weight[:, None] * picked[0] + second_weight[:, None] * picked[1]).astype(BF16)
    return (mixed, gate_new, up_new, down_new)


def solution(mesh):
    return jax.shard_map(
        body,
        mesh=mesh,
        in_specs=(
            P("fs", None),
            P("fs", None),
            P("fs", None),
            P("fs"),
            P(None, "fs", "tp"),
            P(None, "fs", "tp"),
            P(None, "fs", "tp"),
        ),
        out_specs=(P("fs", None), P("fs", None, "tp"), P("fs", None, "tp"), P("fs", None, "tp")),
        check_vma=False,
    )
```

time: 483 us -> 285 us (0.59)
  Pallas kernels: 0 us -> 262 us
  waiting for transfers between devices: 211 us -> 0 us
  blocking collectives: 144 us -> 0 us
  starting transfers between devices: 32.3 us -> 0 us
  local copies, waits for them, and re-layouts: 43.4 us -> 11.7 us
  matrix products: 20.8 us -> 6.58 us
  other arithmetic: 17.3 us -> 3.59 us
  between operations: 13.9 us -> 0.75 us
    pallas_call x0 -> x1, Pallas kernels: none -> 262 us  [body(): pl.pallas_call(functools.partial(handoff, experts, copies, tps), out_shap...]
    all_to_all x3 -> x0, waiting for transfers between devices: 154 us -> none  [the longest x1 75.7 us: body(): lax.all_to_all(up_send, 'fs', split_axis=0, concat_axis=1, tiled=True)]
    all_to_all x2 -> x0, blocking collectives: 144 us -> none  [the longest x1 101 us: body(): lax.all_to_all(gate_send, 'fs', split_axis=0, concat_axis=1, tiled=True)]
    all_to_all x3 -> x0, starting transfers between devices: 32 us -> none  [the longest x1 19.4 us: body(): lax.all_to_all(down_send, 'fs', split_axis=0, concat_axis=1, tiled=True)]
    all_gather x2 -> x0, waiting for transfers between devices: 29.1 us -> none  [the longest x1 16.2 us: body(): piece = lax.all_gather(arrived, 'tp', axis=1, tiled=True)]
    reduce_scatter x1 -> x0, waiting for transfers between devices: 27.1 us -> none  [body(): lax.psum_scatter(partial_value.astype(jnp.bfloat16), 'tp', scatter_dimens...]
    dot_general x2 -> x4, matrix products: 20.8 us -> 6.58 us  [the longest x2 4.6 us: body(): jnp.dot((slot[k][:, None] == slot_ids[None, :]).astype(BF16), returned, p...]
    convert_element_type x5 -> x0, other arithmetic: 12.7 us -> none  [the longest x1 6.12 us: body(): (scaled_gain * up_weight).astype(jnp.bfloat16)]
  transfers between devices with their start and end apart: 6 -> 0, of which waited for: 6 -> 0; matrix products, arithmetic and copies ran while one was open for 4% -> 0% of each run, Pallas kernels for 0% -> 0%
where the time goes in v1:
time: 285 us
  Pallas kernels  262 us (92%)
  local copies, waits for them, and re-layouts  11.7 us (4%)
  matrix products  6.58 us (2%)
  other arithmetic  3.59 us (1%)
    pallas_call x1, Pallas kernels, body(): pl.pallas_call(functools.partial(handoff, experts, copies, tps), out_shap...  262 us
    unnamed x19, local copies, waits for them, and re-layouts  10.2 us

profile of v1, /device:TPU:1, one launch (start us, length us, event | category | flops | bytes accessed | tf_op | source)
XLA Modules:
  0.0 285.1 jit_solution(18424898509674158080)
XLA Ops:
  0.6 0.8 fusion.17
  1.4 0.2 select_reduce_fusion.1
  1.6 0.0 copy-start.4
  1.6 0.0 copy-start.6
  1.6 1.3 convert_reduce_fusion
  2.9 1.5 multiply_reduce_fusion
  4.4 0.0 copy-start.7
  4.4 0.0 copy-done.4
  4.5 0.0 copy-done.6
  4.5 1.8 convolution_convert_fusion.tok
  6.3 0.0 copy-done.7
  6.3 0.7 copy.11.gain
  7.0 262.4 %handoff.1 = (bf16[1,2048,1024]{2,1,0:T(8,128)(2,1)}, bf16[1,2048,1024]{2,1,0:T(8,128)(2,1)}, bf16[1,2048,1024]{2,1,0:T(8,128)(2,1)}, bf16[768,2048]{1,0:T(8,128)(2,1)}) custom-call(bf16[768,1024]{1,0:T(8,128)(2,1)} %convolution_convert_fusion.tok, f32[128,1]{1,0:T(8,128)} %copy.11.gain, f32[8,128,1024]{2,1,0:T(8,128)} %gate_in.1, f32[8,128,1024]{2,1,0:T(8,128)} %up_in.1, ...), custom_call_target="tpu_custom_call" | custom-call | tf_op jit(solution)/shard_map/handoff/pallas_call | solution.py:390
  269.5 0.8 add_divide_fusion
  270.2 0.0 copy-start
  270.2 0.0 copy-start.5
  270.3 2.9 %convolution_multiply_fusion.1 = f32[192,2048]{1,0:T(8,128)S(1)} fusion(bf16[768,2048]{1,0:T(8,128)(2,1)} %get-tuple-element.8, f32[192]{0:T(256)S(1)} %bitcast.8, s32[192]{0:T(256)} %copy-done.6), kind=kOutput, calls=%fused_computation.2 | convolution fusion | flops 604520448 | bytes 4720128 | tf_op jit(solution)/shard_map/dot_general | solution.py:435
  273.1 0.0 copy-done
  273.2 0.0 copy-done.5
  273.2 0.0 copy-start.3
  273.2 1.7 fusion.1
  274.9 0.7 copy-done.3
  275.6 0.0 copy-start.2
  275.6 2.1 copy.15
  277.8 1.6 copy-done.2
  279.3 0.0 copy-start.1
  279.3 2.1 copy.16
  281.5 1.6 copy-done.1
  283.0 2.0 copy.17
  (3 shorter events, 0.0 us)
Async XLA Ops:
  1.6 2.9 %copy-start.4 = (s32[192]{0:T(256)}, s32[192]{0:T(256)S(1)}, u32[]{:S(2)}) copy-start(s32[192]{0:T(256)S(1)} %get-tuple-element.13) | copy-start | bytes 2308
  1.6 2.9 %copy-start.6 = (s32[192]{0:T(256)}, s32[192]{0:T(256)S(1)}, u32[]{:S(2)}) copy-start(s32[192]{0:T(256)S(1)} %get-tuple-element.12) | copy-start | bytes 2308
  4.4 1.8 copy-start.7
  270.2 2.9 %copy-start = (bf16[768,2048]{1,0:T(8,128)(2,1)S(1)}, bf16[768,2048]{1,0:T(8,128)(2,1)}, u32[]{:S(2)}) copy-start(bf16[768,2048]{1,0:T(8,128)(2,1)} %get-tuple-element.8) | copy-start | bytes 9437188
  270.2 2.9 %copy-start.5 = (s32[192]{0:T(256)S(1)}, s32[192]{0:T(256)}, u32[]{:S(2)}) copy-start(s32[192]{0:T(256)} %copy-done.4) | copy-start | bytes 2308
  273.2 2.5 copy-start.3
  275.6 3.7 %copy-start.2 = (bf16[1,2048,1024]{2,1,0:T(8,128)(2,1)S(1)}, bf16[1,2048,1024]{2,1,0:T(8,128)(2,1)}, u32[]{:S(2)}) copy-start(bf16[1,2048,1024]{2,1,0:T(8,128)(2,1)} %get-tuple-element.26) | copy-start | bytes 12582916
  279.3 3.7 %copy-start.1 = (bf16[1,2048,1024]{2,1,0:T(8,128)(2,1)S(1)}, bf16[1,2048,1024]{2,1,0:T(8,128)(2,1)}, u32[]{:S(2)}) copy-start(bf16[1,2048,1024]{2,1,0:T(8,128)(2,1)} %get-tuple-element.27) | copy-start | bytes 12582916

commit v2 on v1

--- a/solution.py
+++ b/solution.py
@@ -8,6 +8,7 @@
 from jax.sharding import PartitionSpec as P
 
 CAP = 96
+STRIDE = 1
 MESH = pl.DeviceIdType.MESH
 BF16 = jnp.bfloat16
 F32 = jnp.float32
@@ -57,8 +58,8 @@
     width = rows_in.shape[1]
     block = tok.shape[1]
     chunk_f = min(256, cols)
-    chunk_w = min(256, block)
-    n_f, n_w = cols // chunk_f, block // chunk_w
+    chunk_w = width // experts
+    n_f, n_w = cols // chunk_f, experts // tps
     me = lax.axis_index("fs")
     tp = lax.axis_index("tp")
     group = lax.div(me, copies)
@@ -66,10 +67,16 @@
     weights = (gate_in, up_in, down_in)
     outs = (gate_out, up_out, down_out)
 
+    paired = experts & (experts - 1) == 0
+
     def ahead(d):
+        if paired:
+            return lax.bitwise_xor(group, lax.rem(jnp.int32(d) * STRIDE, experts))
         return lax.rem(group + d, experts)
 
     def behind(d):
+        if paired:
+            return ahead(d)
         return lax.rem(group + experts - d, experts)
 
     def twin(c):
@@ -147,15 +154,19 @@
             mate(p),
         )
 
-    def partial(p, j):
-        where = pl.ds(pl.multiple_of(j * chunk_w, 128), chunk_w)
-        return remote(
-            part.at[p - 1, :, where],
-            part_in.at[p - 1, :, where],
-            p_send.at[p, j],
+    def features(e):
+        return pl.ds(pl.multiple_of(e * chunk_w, 128), chunk_w)
+
+    def partial(e, q):
+        owner, j = lax.div(e, n_w), lax.rem(e, n_w)
+        p = lax.rem(owner - q + tps, tps)
+        return remote(
+            part.at[:, features(e)],
+            part_in.at[p - 1, :, features(j)],
+            p_send.at[e],
             p_recv.at[p, j],
             me,
-            mate(p),
+            owner,
         )
 
     def give(s, e, j):
@@ -249,9 +260,6 @@
     loop(1, experts, spread_step)
     loop(1, experts, lambda d: relay_step(0, d))
     loop(1, experts, lambda d: relay_step(1, d))
-    early = experts - n_f
-    loop(1, early, lambda d: relay_step(2, d))
-
     def spread_wait(s):
         for p in range(1, tps):
             spread(s, mate(tps - p), p).wait_recv()
@@ -262,43 +270,56 @@
         out_copy(m).start()
 
     def gate_up(c):
-        relay_step(2, early + c)
+        @pl.when(c < experts - 1)
+        def _():
+            relay_step(2, 1 + c)
+
         where = pl.ds(pl.multiple_of(c * chunk_f, 128), chunk_f)
         gate = jnp.dot(rows_in[...], full[0, :, where], preferred_element_type=F32)
         up = jnp.dot(rows_in[...], full[1, :, where], preferred_element_type=F32)
         hidden[:, where] = (gate / (1.0 + jnp.exp(-gate)) * up).astype(BF16)
 
     loop(0, n_f, gate_up)
-    loop(0, experts, lambda s: relay_wait(2, s))
+    def add_up(e):
+        @pl.when(lax.div(e, n_w) == tp)
+        def _():
+            j = lax.rem(e, n_w)
+            total = part[:, features(e)].astype(F32)
+            for p in range(1, tps):
+                partial(e, mate(tps - p)).wait_recv()
+                total = total + part_in[p - 1, :, features(j)].astype(F32)
+            share[:, features(j)] = total.astype(BF16)
+            back[slots(group), features(e)] = share[slots(group), features(j)]
+            loop(1, experts, lambda d: give(behind(d), group, j).start())
+            for p in range(1, tps):
+                fan(group, tp, j, p).start()
+
+    def down_step(d):
+        e = behind(d)
+
+        @pl.when(d + n_f < experts - 1)
+        def _():
+            relay_step(2, d + n_f + 1)
+
+        relay_wait(2, e)
+        part[:, features(e)] = lax.dot_general(
+            hidden[...],
+            full[2, features(e), :],
+            (((1,), (1,)), ((), ())),
+            preferred_element_type=F32,
+        ).astype(BF16)
+
+        @pl.when(lax.div(e, n_w) != tp)
+        def _():
+            partial(e, tp).start()
+
+        @pl.when(d > 0)
+        def _():
+            add_up(behind(d - 1))
+
+    loop(0, experts, down_step)
     out_copy(2).start()
-
-    def down(q, j):
-        rows = full[2, own_cols(q, j, chunk_w), :]
-        return lax.dot_general(
-            hidden[...], rows, (((1,), (1,)), ((), ())), preferred_element_type=F32
-        ).astype(BF16)
-
-    for p in range(1, tps):
-        def partial_step(j, p=p):
-            where = pl.ds(pl.multiple_of(j * chunk_w, 128), chunk_w)
-            part[p - 1, :, where] = down(mate(p), j)
-            partial(p, j).start()
-
-        loop(0, n_w, partial_step)
-
-    def share_step(j):
-        where = pl.ds(pl.multiple_of(j * chunk_w, 128), chunk_w)
-        total = down(tp, j).astype(F32)
-        for p in range(1, tps):
-            partial(p, j).wait_recv()
-            total = total + part_in[p - 1, :, where].astype(F32)
-        share[:, where] = total.astype(BF16)
-        back[slots(group), own_cols(tp, j, chunk_w)] = share[slots(group), where]
-        loop(1, experts, lambda d: give(behind(d), group, j).start())
-        for p in range(1, tps):
-            fan(group, tp, j, p).start()
-
-    loop(0, n_w, share_step)
+    add_up(behind(experts - 1))
 
     def back_step(j):
         def one(d):
@@ -339,9 +360,14 @@
 
     loop(0, experts, spreads)
 
+    def part_sent(e):
+        @pl.when(lax.div(e, n_w) != tp)
+        def _():
+            partial(e, tp).wait_send()
+
+    loop(0, experts, part_sent)
+
     def tail(j):
-        for p in range(1, tps):
-            partial(p, j).wait_send()
         loop(1, experts, lambda d: give(behind(d), group, j).wait_send())
 
         def fans(e):
@@ -383,7 +409,7 @@
     mine = lax.dynamic_slice_in_dim(normed, lax.axis_index("tp") * block, block, 1)
     tok = jnp.dot(scatter, mine, preferred_element_type=F32).astype(BF16)
 
-    n_w = block // min(256, block)
+    n_w = experts // tps
     dma = pltpu.SemaphoreType.DMA
     anywhere = pl.BlockSpec(memory_space=pl.ANY)
     copy_shape = jax.ShapeDtypeStruct((1, depth, cols), BF16)
@@ -403,7 +429,7 @@
             pltpu.VMEM((3, depth, cols), BF16),
             pltpu.VMEM((n_slots, width), BF16),
             pltpu.VMEM((n_slots, cols), BF16),
-            pltpu.VMEM((tps - 1, n_slots, block), BF16),
+            pltpu.VMEM((n_slots, width), BF16),
             pltpu.VMEM((tps - 1, n_slots, block), BF16),
             pltpu.VMEM((n_slots, block), BF16),
             pltpu.VMEM((n_slots, width), BF16),
@@ -416,7 +442,7 @@
             dma((experts,)),
             dma((experts, tps)),
             dma((experts, tps)),
-            dma((tps, n_w)),
+            dma((experts,)),
             dma((tps, n_w)),
             dma((experts, n_w)),
             dma((experts, n_w)),

time: 285 us -> 245 us (0.86)
  Pallas kernels: 262 us -> 222 us
    pallas_call x1, Pallas kernels: 262 us -> 222 us  [body(): pl.pallas_call(functools.partial(handoff, experts, copies, tps), out_shap...]
where the time goes in v2:
time: 245 us
  Pallas kernels  222 us (91%)
  local copies, waits for them, and re-layouts  11.7 us (5%)
  matrix products  6.59 us (3%)
  other arithmetic  3.59 us (1%)
    pallas_call x1, Pallas kernels, body(): pl.pallas_call(functools.partial(handoff, experts, copies, tps), out_shap...  222 us
    unnamed x19, local copies, waits for them, and re-layouts  10.2 us

profile of v2, /device:TPU:1, one launch (start us, length us, event | category | flops | bytes accessed | tf_op | source)
XLA Modules:
  0.0 244.8 jit_solution(7990059401107350101)
XLA Ops:
  0.6 0.8 fusion.17
  1.4 0.2 select_reduce_fusion.1
  1.6 0.0 copy-start.4
  1.6 0.0 copy-start.6
  1.6 1.3 convert_reduce_fusion
  2.9 1.5 multiply_reduce_fusion
  4.4 0.0 copy-start.7
  4.4 0.0 copy-done.4
  4.5 0.0 copy-done.6
  4.5 1.8 convolution_convert_fusion.tok
  6.3 0.0 copy-done.7
  6.3 0.7 copy.11.gain
  7.0 222.2 %handoff.1 = (bf16[1,2048,1024]{2,1,0:T(8,128)(2,1)}, bf16[1,2048,1024]{2,1,0:T(8,128)(2,1)}, bf16[1,2048,1024]{2,1,0:T(8,128)(2,1)}, bf16[768,2048]{1,0:T(8,128)(2,1)}) custom-call(bf16[768,1024]{1,0:T(8,128)(2,1)} %convolution_convert_fusion.tok, f32[128,1]{1,0:T(8,128)} %copy.11.gain, f32[8,128,1024]{2,1,0:T(8,128)} %gate_in.1, f32[8,128,1024]{2,1,0:T(8,128)} %up_in.1, ...), custom_call_target="tpu_custom_call" | custom-call | tf_op jit(solution)/shard_map/handoff/pallas_call | solution.py:416
  229.3 0.8 add_divide_fusion
  230.0 0.0 copy-start
  230.0 0.0 copy-start.5
  230.0 2.9 %convolution_multiply_fusion.1 = f32[192,2048]{1,0:T(8,128)S(1)} fusion(bf16[768,2048]{1,0:T(8,128)(2,1)} %get-tuple-element.8, f32[192]{0:T(256)S(1)} %bitcast.8, s32[192]{0:T(256)} %copy-done.6), kind=kOutput, calls=%fused_computation.2 | convolution fusion | flops 604520448 | bytes 4720128 | tf_op jit(solution)/shard_map/dot_general | solution.py:461
  232.9 0.0 copy-done
  232.9 0.0 copy-done.5
  233.0 0.0 copy-start.3
  233.0 1.7 fusion.1
  234.7 0.7 copy-done.3
  235.4 0.0 copy-start.2
  235.4 2.1 copy.15
  237.6 1.6 copy-done.2
  239.1 0.0 copy-start.1
  239.1 2.1 copy.16
  241.3 1.6 copy-done.1
  242.8 2.0 copy.17
  (3 shorter events, 0.0 us)
Async XLA Ops:
  1.6 2.9 %copy-start.4 = (s32[192]{0:T(256)}, s32[192]{0:T(256)S(1)}, u32[]{:S(2)}) copy-start(s32[192]{0:T(256)S(1)} %get-tuple-element.13) | copy-start | bytes 2308
  1.6 2.9 %copy-start.6 = (s32[192]{0:T(256)}, s32[192]{0:T(256)S(1)}, u32[]{:S(2)}) copy-start(s32[192]{0:T(256)S(1)} %get-tuple-element.12) | copy-start | bytes 2308
  4.4 1.8 copy-start.7
  230.0 2.9 %copy-start = (bf16[768,2048]{1,0:T(8,128)(2,1)S(1)}, bf16[768,2048]{1,0:T(8,128)(2,1)}, u32[]{:S(2)}) copy-start(bf16[768,2048]{1,0:T(8,128)(2,1)} %get-tuple-element.8) | copy-start | bytes 9437188
  230.0 2.9 %copy-start.5 = (s32[192]{0:T(256)S(1)}, s32[192]{0:T(256)}, u32[]{:S(2)}) copy-start(s32[192]{0:T(256)} %copy-done.4) | copy-start | bytes 2308
  233.0 2.5 %copy-start.3 = (bf16[1,2048,1024]{2,1,0:T(8,128)(2,1)S(1)}, bf16[1,2048,1024]{2,1,0:T(8,128)(2,1)}, u32[]{:S(2)}) copy-start(bf16[1,2048,1024]{2,1,0:T(8,128)(2,1)} %get-tuple-element.25) | copy-start | bytes 12582916
  235.4 3.7 %copy-start.2 = (bf16[1,2048,1024]{2,1,0:T(8,128)(2,1)S(1)}, bf16[1,2048,1024]{2,1,0:T(8,128)(2,1)}, u32[]{:S(2)}) copy-start(bf16[1,2048,1024]{2,1,0:T(8,128)(2,1)} %get-tuple-element.26) | copy-start | bytes 12582916
  239.1 3.7 %copy-start.1 = (bf16[1,2048,1024]{2,1,0:T(8,128)(2,1)S(1)}, bf16[1,2048,1024]{2,1,0:T(8,128)(2,1)}, u32[]{:S(2)}) copy-start(bf16[1,2048,1024]{2,1,0:T(8,128)(2,1)} %get-tuple-element.27) | copy-start | bytes 12582916
